TPU v7x, 512 devices: a whole 4x4x16 slice. The times are simulated.
512 devices in a mesh: sp: 64 (over z, y), tp: 8 (over x, core).
Axes of the slice: x: 4, y: 4, z: 16, core: 2. Of those that a mesh axis runs over, the one named last changes fastest.
Arguments:
- stream: bfloat16 [8192, 2048], P('sp'), may hold values from -6 to 6
- query_narrow: bfloat16 [8192, 512], P('sp', 'tp'), may hold values from -7 to 7
- query_broad: bfloat16 [8192, 1024], P('sp', 'tp'), may hold values from -7 to 7
- key_narrow: bfloat16 [8192, 512], P('sp', 'tp'), may hold values from -7 to 7
- key_broad: bfloat16 [8192, 1024], P('sp', 'tp'), may hold values from -7 to 7
- value_narrow: bfloat16 [8192, 512], P('sp', 'tp'), may hold values from -6 to 6
- value_broad: bfloat16 [8192, 1024], P('sp', 'tp'), may hold values from -6 to 6
- key_offsets: float32 [8192, 16], P('sp', 'tp'), may hold values from -20 to 0
- out_narrow: bfloat16 [512, 2048], P('tp'), may hold values from -0.4375 to 0.4375
- out_broad: bfloat16 [1024, 2048], P('tp'), may hold values from -0.4375 to 0.4375
- norm_gain: float32 [2048], replicated, may hold values from 0.1 to 1.9
- gate_weight: bfloat16 [2048, 3072], P('sp', 'tp'), may hold values from -0.125 to 0.125
- up_weight: bfloat16 [2048, 3072], P('sp', 'tp'), may hold values from -0.125 to 0.125
- down_weight: bfloat16 [3072, 2048], P('tp', 'sp'), may hold values from -0.21875 to 0.21875
Outputs:
- result: bfloat16 [8192, 2048], P(('sp', 'tp'))
All inputs are finite; a program needn't handle non-finite values.
Results may differ from a plain program's by a relative error of at most 0.028.
Values may be sent and summed in bfloat16 or wider, within the bound.
A program may use at most 64 MiB of HBM per device.

v0:
```python
import jax
import jax.numpy as jnp
from jax import lax
from jax.sharding import Mesh
from jax.sharding import PartitionSpec as P

NARROW_SIZE = 64
BROAD_SIZE = 128
SP = ("sp_0", "sp_1")
SP_TP = ("sp_0", "sp_1", "tp")
grain = 8
block_keys = 512
norm_eps = 1e-06


def laid_out(blocks, dim):
    blocks = jnp.moveaxis(blocks, 0, dim)
    shape = blocks.shape
    return blocks.reshape(*shape[:dim], shape[dim] * shape[dim + 1], *shape[dim + 2 :])


def gather_in_order(shard, axes, sequence):
    blocks = shard[None]
    for k in sequence:
        blocks = lax.all_gather(blocks, axes[k], axis=0, tiled=True)
    carried = [lax.axis_size(axes[k]) for k in reversed(sequence)]
    blocks = blocks.reshape(*carried, *shard.shape)
    turned = sorted(range(len(sequence)), key=lambda place: sequence[len(sequence) - 1 - place])
    return blocks.transpose(*turned, *range(len(sequence), blocks.ndim)).reshape(-1, *shard.shape)


def whole_of(shard, axes, sequence, dim):
    return laid_out(gather_in_order(shard, axes, sequence), dim)


def sent_to_all(shard, axis):
    peers = lax.axis_size(axis)
    return lax.all_to_all(
        jnp.broadcast_to(shard[None], (peers, *shard.shape)), axis, 0, 0, tiled=True
    )


def over_copies(shard, axis):
    return sent_to_all(shard, axis).astype(jnp.float32).sum(axis=0)


def in_one_piece(arrays, axis, dim, along):
    widths = [a.shape[along] for a in arrays]
    both = jnp.concatenate(arrays, axis=along)
    filled = lax.all_gather(both, axis, axis=dim, tiled=True)
    return tuple(jnp.split(filled, [sum(widths[:k]) for k in range(1, len(widths))], axis=along))


def gather_axes(shard, axes, dim):
    filled = shard
    for number in range(len(axes) - 1, -1, -1):
        filled = lax.all_gather(filled, axes[number], axis=dim, tiled=True)
    return filled


def cut_along(shard, dim, peers):
    shape = shard.shape
    blocks = shard.reshape(*shape[:dim], peers, shape[dim] // peers, *shape[dim + 1 :])
    return jnp.moveaxis(blocks, dim, 0)


def summed_on_arrival(shard, axis, dim):
    peers = lax.axis_size(axis)
    blocks = lax.all_to_all(cut_along(shard, dim, peers), axis, 0, 0, tiled=True)
    return jnp.sum(blocks.astype(jnp.float32), axis=0)


def block_plan(length):
    return (length // block_keys, block_keys)


def slice_rows(array, first, count):
    return lax.dynamic_slice_in_dim(array, first, count, 0)


def head_logs(queries, keys_block, offset_block, positions, key_positions, scale):
    logits = (
        jnp.einsum("qhd,khd->hqk", queries, keys_block, preferred_element_type=jnp.float32) * scale
    )
    logits = logits + jnp.transpose(offset_block)[:, None, :]
    causal = (key_positions[None, :] < positions[:, None])[None, :, :]
    lognot = jnp.where(causal, jax.nn.log_sigmoid(-logits), 0.0)
    return (logits, causal, lognot)


def sub_totals(lognot):
    heads, count, length = lognot.shape
    return lognot.reshape(heads, count, length // grain, grain).sum(axis=3)


def weighted_values(logits, causal, lognot, after, values):
    heads, count, length = lognot.shape
    grouped = lognot.reshape(heads, count, length // grain, grain)
    within = lax.cumsum(grouped, axis=3, reverse=True) - grouped
    later = (within + after[:, :, :, None]).reshape(heads, count, length)
    weights = jnp.where(causal, jnp.exp(jax.nn.log_sigmoid(logits) + later), 0.0).astype(
        jnp.bfloat16
    )
    return jnp.einsum("hqk,khd->qhd", weights, values, preferred_element_type=jnp.float32)


def local(
    stream,
    query_narrow,
    query_broad,
    key_narrow,
    key_broad,
    value_narrow,
    value_broad,
    key_offsets,
    out_narrow,
    out_broad,
    norm_gain,
    gate_weight,
    up_weight,
    down_weight,
):
    rows = stream.shape[0]
    heads = query_narrow.shape[1] // NARROW_SIZE
    shaped_narrow = query_narrow.reshape(rows, heads, NARROW_SIZE)
    shaped_broad = query_broad.reshape(rows, heads, BROAD_SIZE)
    positions = lax.axis_index(SP) * rows + jnp.arange(rows, dtype=jnp.int32)
    scale_narrow = NARROW_SIZE ** (-0.5)
    scale_broad = BROAD_SIZE ** (-0.5)

    def key_block(keys_narrow, keys_broad, offsets, first, count):
        block_narrow = slice_rows(keys_narrow, first, count).reshape(count, heads, NARROW_SIZE)
        block_broad = slice_rows(keys_broad, first, count).reshape(count, heads, BROAD_SIZE)
        pairs = slice_rows(offsets, first, count).reshape(count, heads, 2)
        return (block_narrow, block_broad, pairs[:, :, 0], pairs[:, :, 1])

    def value_block(values_narrow, values_broad, first, count):
        return (
            slice_rows(values_narrow, first, count).reshape(count, heads, NARROW_SIZE),
            slice_rows(values_broad, first, count).reshape(count, heads, BROAD_SIZE),
        )

    empty_narrow = jnp.zeros((rows, heads, NARROW_SIZE), jnp.float32)
    empty_broad = jnp.zeros((rows, heads, BROAD_SIZE), jnp.float32)
    whole = (
        whole_of(key_narrow, SP, (0, 1), 0),
        whole_of(key_broad, SP, (0, 1), 0),
        whole_of(value_narrow, SP, (0, 1), 0),
        whole_of(value_broad, SP, (0, 1), 0),
        whole_of(key_offsets.astype(jnp.bfloat16), SP, (0, 1), 0).astype(key_offsets.dtype),
    )
    keys_narrow, keys_broad, values_narrow, values_broad, offsets = whole
    steps, span = block_plan(keys_narrow.shape[0])
    running = jnp.zeros((heads, rows), jnp.float32)

    def back_step(index, state):
        first = (steps - 1 - index) * span
        block_narrow, block_broad, offset_narrow, offset_broad = key_block(
            keys_narrow, keys_broad, offsets, first, span
        )
        held_narrow, held_broad = value_block(values_narrow, values_broad, first, span)
        key_positions = first + jnp.arange(span, dtype=jnp.int32)
        logits_narrow, causal_narrow, lognot_narrow = head_logs(
            shaped_narrow, block_narrow, offset_narrow, positions, key_positions, scale_narrow
        )
        logits_broad, causal_broad, lognot_broad = head_logs(
            shaped_broad, block_broad, offset_broad, positions, key_positions, scale_broad
        )
        subs_narrow = sub_totals(lognot_narrow)
        subs_broad = sub_totals(lognot_broad)
        later_narrow = (
            lax.cumsum(subs_narrow, axis=2, reverse=True) - subs_narrow + state[2][:, :, None]
        )
        later_broad = (
            lax.cumsum(subs_broad, axis=2, reverse=True) - subs_broad + state[3][:, :, None]
        )
        return (
            state[0]
            + weighted_values(
                logits_narrow, causal_narrow, lognot_narrow, later_narrow, held_narrow
            ),
            state[1]
            + weighted_values(logits_broad, causal_broad, lognot_broad, later_broad, held_broad),
            state[2] + subs_narrow.sum(axis=2),
            state[3] + subs_broad.sum(axis=2),
        )

    final = lax.fori_loop(0, steps, back_step, (empty_narrow, empty_broad, running, running))
    acc_narrow = final[0]
    acc_broad = final[1]
    attended_narrow = acc_narrow.reshape(rows, heads * NARROW_SIZE).astype(jnp.bfloat16)
    attended_broad = acc_broad.reshape(rows, heads * BROAD_SIZE).astype(jnp.bfloat16)
    share = rows // lax.axis_size("tp")
    own = lax.axis_index("tp") * share
    summed = over_copies(
        (
            jnp.dot(
                slice_rows(attended_narrow, 0, rows), out_narrow, preferred_element_type=jnp.float32
            )
            + jnp.dot(
                slice_rows(attended_broad, 0, rows), out_broad, preferred_element_type=jnp.float32
            )
        ).astype(jnp.bfloat16),
        "tp",
    ).astype(jnp.float32)
    mid_all = (stream.astype(jnp.float32) + summed).astype(jnp.bfloat16)
    middle = mid_all.astype(jnp.float32)
    scaled = middle * lax.rsqrt(jnp.mean(middle * middle, axis=1, keepdims=True) + norm_eps)
    normed = (scaled * norm_gain).astype(jnp.bfloat16)
    mid_own = slice_rows(mid_all, own, share)
    part_gate, part_up = in_one_piece((gate_weight, up_weight), SP, 0, 1)
    gate = jnp.dot(normed, part_gate, preferred_element_type=jnp.float32)
    up = jnp.dot(normed, part_up, preferred_element_type=jnp.float32)
    hidden = (jax.nn.silu(gate) * up).astype(jnp.bfloat16)
    down_full = gather_axes(down_weight, SP, 1)
    mixed = summed_on_arrival(
        jnp.dot(
            slice_rows(hidden, jnp.int32(0), share * lax.axis_size("tp")),
            down_full,
            preferred_element_type=jnp.float32,
        ).astype(jnp.bfloat16),
        "tp",
        0,
    )
    return (mid_own.astype(jnp.float32) + mixed).astype(jnp.bfloat16)


def solution(mesh):
    torus = Mesh(mesh.devices.reshape(16, 4, mesh.shape["tp"]), ("sp_0", "sp_1", "tp"))
    in_specs = (
        P(SP, None),
        P(SP, "tp"),
        P(SP, "tp"),
        P(SP, "tp"),
        P(SP, "tp"),
        P(SP, "tp"),
        P(SP, "tp"),
        P(SP, "tp"),
        P("tp", None),
        P("tp", None),
        P(),
        P(SP, "tp"),
        P(SP, "tp"),
        P("tp", SP),
    )
    out_specs = P(SP_TP, None)
    return jax.shard_map(local, mesh=torus, in_specs=in_specs, out_specs=out_specs, check_vma=False)
```

profile of v0, /device:TPU:1, one launch (start us, length us, event | category | flops | bytes accessed | tf_op | source)
XLA Modules:
  0.0 433.5 jit_solution(11852103382589410577)
XLA Ops:
  6.6 30.8 %all-gather = bf16[2048,64]{0,1:T(8,128)(2,1)S(1)} all-gather(bf16[128,64]{0,1:T(8,128)(2,1)} %param.21), channel_id=2, replica_groups=mesh['sp_0'=16,'sp_1'=4,'tp'=8] {'sp_0'}, dimensions={0}, use_global_device_ids=true | all-gather | bytes 278528 | tf_op jit(solution)/shard_map/all_gather | solution.py:25
  38.2 21.0 %all-gather.1 = bf16[2048,64]{0,1:T(8,128)(2,1)S(1)} all-gather(bf16[128,64]{0,1:T(8,128)(2,1)} %param.19), channel_id=3, replica_groups=mesh['sp_0'=16,'sp_1'=4,'tp'=8] {'sp_0'}, dimensions={0}, use_global_device_ids=true | all-gather | bytes 278528 | tf_op jit(solution)/shard_map/all_gather | solution.py:25
  60.1 26.6 %all-gather.3 = bf16[2048,128]{1,0:T(8,128)(2,1)} all-gather(bf16[128,128]{1,0:T(8,128)(2,1)S(1)} %copy-done.4), channel_id=5, replica_groups=mesh['sp_0'=16,'sp_1'=4,'tp'=8] {'sp_0'}, dimensions={0}, use_global_device_ids=true | all-gather | bytes 557056 | tf_op jit(solution)/shard_map/all_gather | solution.py:25
  86.7 25.8 %all-gather.4 = bf16[2048,128]{1,0:T(8,128)(2,1)} all-gather(bf16[128,128]{1,0:T(8,128)(2,1)S(1)} %copy-done.5), channel_id=6, replica_groups=mesh['sp_0'=16,'sp_1'=4,'tp'=8] {'sp_0'}, dimensions={0}, use_global_device_ids=true | all-gather | bytes 557056 | tf_op jit(solution)/shard_map/all_gather | solution.py:25
  113.4 19.6 %all-gather.2 = bf16[2048,2]{0,1:T(2,128)(2,1)S(1)} all-gather(bf16[128,2]{0,1:T(2,128)(2,1)S(1)} %convert_element_type.77), channel_id=4, replica_groups=mesh['sp_0'=16,'sp_1'=4,'tp'=8] {'sp_0'}, dimensions={0}, use_global_device_ids=true | all-gather | bytes 8704 | tf_op jit(solution)/shard_map/all_gather | solution.py:25
  132.9 12.1 %all_gather.44 = bf16[64,128,2]{1,0,2:T(8,128)(2,1)S(1)} all-gather(bf16[16,128,2]{1,0,2:T(8,128)(2,1)S(1)} %bitcast.157), channel_id=1, replica_groups=mesh['sp_0'=16,'sp_1'=4,'tp'=8] {'sp_1'}, dimensions={0}, use_global_device_ids=true | all-gather | bytes 40960 | tf_op jit(solution)/shard_map/all_gather | solution.py:25
  145.1 3.1 copy.44
  148.3 3.1 copy.46
  152.4 3.2 copy.39
  155.6 37.4 %all-gather.18.cloned.1.call-done = bf16[64,128,128]{2,1,0:T(8,128)(2,1)} async-done(((bf16[16,128,128]{2,1,0:T(8,128)(2,1)}), bf16[64,128,128]{2,1,0:T(8,128)(2,1)}) %all-gather.18.cloned.1.call-update) | async-done | bytes 2097168 | tf_op jit(solution)/shard_map/all_gather | solution.py:25
  193.0 3.3 copy.40
  196.3 116.7 %while.20 = (s32[]{:T(128)}, f32[128,1,64]{0,2,1:T(8,128)S(1)}, f32[128,1,128]{0,2,1:T(8,128)S(1)}, f32[1,128]{1,0:T(1,128)S(1)}, f32[1,128]{1,0:T(1,128)S(1)}, ...) while((s32[]{:T(128)}, f32[128,1,64]{0,2,1:T(8,128)S(1)}, ...), condition=%wide.region_9.10_spmd.clone, body=%wide.region_0.9_spmd.clone.sunk | while | flops 57983880 | bytes 5200671 | solution.py:188
  214.6 1.5 fusion.94
  309.4 1.5 fusion.94
  313.7 2.5 broadcast_in_dim.69
  316.2 5.4 %all-to-all-start = ((bf16[8,128,2048]{2,1,0:T(8,128)(2,1)}), bf16[8,128,2048]{2,1,0:T(8,128)(2,1)}, u32[]{:S(2)}, u32[]{:S(2)}) async-start(bf16[8,128,2048]{2,1,0:T(8,128)(2,1)} %broadcast_in_dim.69), calls=%async_computation | async-start | bytes 8388608 | tf_op jit(solution)/shard_map/all_to_all | solution.py:38
  321.6 10.7 %all_gather.50 = bf16[384,128]{0,1:T(8,128)(2,1)} all-gather(bf16[384,32]{0,1:T(8,128)(2,1)S(1)} %copy-done.8), channel_id=1, replica_groups=mesh['sp_0'=16,'sp_1'=4,'tp'=8] {'sp_1'}, dimensions={1}, use_global_device_ids=true | all-gather | bytes 122880 | tf_op jit(solution)/shard_map/all_gather | solution.py:57
  332.3 38.1 %all-to-all-done = bf16[8,128,2048]{2,1,0:T(8,128)(2,1)} async-done(((bf16[8,128,2048]{2,1,0:T(8,128)(2,1)}), bf16[8,128,2048]{2,1,0:T(8,128)(2,1)}, u32[]{:S(2)}, u32[]{:S(2)}) %all-to-all-start) | async-done | bytes 4194336 | tf_op jit(solution)/shard_map/all_to_all | solution.py:38
  370.4 3.0 convert_reduce_fusion
  374.1 1.9 fusion.41
  376.0 23.2 %all-gather.22.cloned.1.call-done = bf16[384,2048]{0,1:T(8,128)(2,1)} async-done(((bf16[384,128]{0,1:T(8,128)(2,1)}), bf16[384,2048]{0,1:T(8,128)(2,1)}) %all-gather.22.cloned.1.call-update) | async-done | bytes 1572880 | tf_op jit(solution)/shard_map/all_gather | solution.py:57
  399.3 3.7 convolution_convert_fusion
  403.0 13.6 %all-to-all-start.1 = ((bf16[8,16,2048]{2,1,0:T(8,128)(2,1)}), bf16[8,16,2048]{2,1,0:T(8,128)(2,1)S(1)}, u32[]{:S(2)}, u32[]{:S(2)}) async-start(bf16[8,16,2048]{2,1,0:T(8,128)(2,1)} %bitcast.22), calls=%async_computation.1 | async-start | bytes 1048576 | tf_op jit(solution)/shard_map/all_to_all | solution.py:69
  416.6 9.3 %all-to-all-done.1 = bf16[8,16,2048]{2,1,0:T(8,128)(2,1)S(1)} async-done(((bf16[8,16,2048]{2,1,0:T(8,128)(2,1)}), bf16[8,16,2048]{2,1,0:T(8,128)(2,1)S(1)}, u32[]{:S(2)}, u32[]{:S(2)}) %all-to-all-start.1) | async-done | bytes 524320 | tf_op jit(solution)/shard_map/all_to_all | solution.py:69
  (312 shorter events, 117.8 us)
Async XLA Ops:
  6.5 306.8 %copy-start = (bf16[128,2048]{1,0:T(8,128)(2,1)S(1)}, bf16[128,2048]{1,0:T(8,128)(2,1)}, u32[]{:S(2)}) copy-start(bf16[128,2048]{1,0:T(8,128)(2,1)} %param.25) | copy-start | bytes 1572868
  6.5 53.5 %copy-start.4 = (bf16[128,128]{1,0:T(8,128)(2,1)S(1)}, bf16[128,128]{1,0:T(8,128)(2,1)}, u32[]{:S(2)}) copy-start(bf16[128,128]{1,0:T(8,128)(2,1)} %param.22) | copy-start | bytes 98308
  6.5 80.2 %copy-start.5 = (bf16[128,128]{1,0:T(8,128)(2,1)S(1)}, bf16[128,128]{1,0:T(8,128)(2,1)}, u32[]{:S(2)}) copy-start(bf16[128,128]{1,0:T(8,128)(2,1)} %param.20) | copy-start | bytes 98308
  6.5 106.1 %copy-start.7 = (bf16[32,384]{1,0:T(8,128)(2,1)S(1)}, bf16[32,384]{1,0:T(8,128)(2,1)}, u32[]{:S(2)}) copy-start(bf16[32,384]{1,0:T(8,128)(2,1)} %param.27) | copy-start | bytes 73732
  6.5 106.1 %copy-start.6 = (bf16[32,384]{1,0:T(8,128)(2,1)S(1)}, bf16[32,384]{1,0:T(8,128)(2,1)}, u32[]{:S(2)}) copy-start(bf16[32,384]{1,0:T(8,128)(2,1)} %param.28) | copy-start | bytes 73732
  6.5 138.6 %all-gather.12.cloned.1.call-start = ((), (), s32[]{:S(2)}) async-start(), calls=%async_computation.2 | async-start | bytes 1310720 | tf_op jit(solution)/shard_map/all_gather | solution.py:25
  37.4 75.9 %copy-start.11 = (f32[128,2]{0,1:T(2,128)S(1)}, f32[128,2]{0,1:T(2,128)}, u32[]{:S(2)}) copy-start(f32[128,2]{0,1:T(2,128)} %param.23) | copy-start | bytes 3076
  38.2 110.1 %all-gather.14.cloned.1.call-start = ((), (), s32[]{:S(2)}) async-start(), calls=%async_computation.3 | async-start | bytes 1310720 | tf_op jit(solution)/shard_map/all_gather | solution.py:25
  60.0 92.4 %all-gather.16.cloned.1.call-start = ((), (), s32[]{:S(2)}) async-start(), calls=%async_computation.4 | async-start | bytes 2621440 | tf_op jit(solution)/shard_map/all_gather | solution.py:25
  86.6 106.3 %all-gather.18.cloned.1.call-start = ((), (), s32[]{:S(2)}) async-start(), calls=%async_computation.5 | async-start | bytes 2621440 | tf_op jit(solution)/shard_map/all_gather | solution.py:25
  112.6 261.2 %all-gather.20.cloned.1.call-start = ((), (), s32[]{:S(2)}) async-start(), calls=%async_computation.6 | async-start | bytes 3194880 | tf_op jit(solution)/shard_map/all_gather | solution.py:50
  193.0 3.3 copy-start.2
  193.0 3.3 copy-start.9
  196.3 116.7 %copy-start.3 = (bf16[64,2048]{1,0:T(8,128)(2,1)S(1)}, bf16[64,2048]{1,0:T(8,128)(2,1)}, u32[]{:S(2)}) copy-start(bf16[64,2048]{1,0:T(8,128)(2,1)} %param.24) | copy-start | bytes 786436
  316.2 5.4 %copy-start.8 = (bf16[384,32]{0,1:T(8,128)(2,1)S(1)}, bf16[384,32]{0,1:T(8,128)(2,1)}, u32[]{:S(2)}) copy-start(bf16[384,32]{0,1:T(8,128)(2,1)} %param.29) | copy-start | bytes 73732
  316.2 54.2 %all-to-all-start = ((bf16[8,128,2048]{2,1,0:T(8,128)(2,1)}), bf16[8,128,2048]{2,1,0:T(8,128)(2,1)}, u32[]{:S(2)}, u32[]{:S(2)}) async-start(bf16[8,128,2048]{2,1,0:T(8,128)(2,1)} %broadcast_in_dim.69), calls=%async_computation | async-start | bytes 8388608 | tf_op jit(solution)/shard_map/all_to_all | solution.py:38
  321.6 77.7 %all-gather.22.cloned.1.call-start = ((), (), s32[]{:S(2)}) async-start(), calls=%async_computation.7 | async-start | bytes 1671168 | tf_op jit(solution)/shard_map/all_gather | solution.py:57
  332.3 41.1 %copy-start.1 = (bf16[128,2048]{1,0:T(8,128)(2,1)S(1)}, bf16[128,2048]{1,0:T(8,128)(2,1)}, u32[]{:S(2)}) copy-start(bf16[128,2048]{1,0:T(8,128)(2,1)} %param.16) | copy-start | bytes 1572868
  373.4 0.7 copy-start.10
  403.0 23.0 %all-to-all-start.1 = ((bf16[8,16,2048]{2,1,0:T(8,128)(2,1)}), bf16[8,16,2048]{2,1,0:T(8,128)(2,1)S(1)}, u32[]{:S(2)}, u32[]{:S(2)}) async-start(bf16[8,16,2048]{2,1,0:T(8,128)(2,1)} %bitcast.22), calls=%async_computation.1 | async-start | bytes 1048576 | tf_op jit(solution)/shard_map/all_to_all | solution.py:69
Sparse Core Ops, SparseCore 0:
  38.3 34.8 all-gather.11
  75.3 33.8 all-gather.13
  111.3 41.0 all-gather.15
  154.4 38.5 all-gather.17
  195.8 134.4 all-gather.19
  332.4 66.7 all-gather.21
where the time goes:
time: 435 us; the launch traced here: 434 us
  blocking collectives  146 us (34%)
  waiting for transfers between devices  109 us (25%)
  matrix products  93 us (21%)
  other arithmetic  32.7 us (8%)
  starting transfers between devices  19.2 us (4%)
  local copies, waits for them, and re-layouts  17.6 us (4%)
  between operations  13.7 us (3%)
    all_gather x6, blocking collectives, gather_in_order(): blocks = lax.all_gather(blocks, axes[k], axis=0, tiled=True)  136 us
    dot_general x32, matrix products, weighted_values(): jnp.einsum('hqk,khd->qhd', weights, values, preferred_element_type=jnp.fl...  46.6 us
    dot_general x32, matrix products, head_logs(): jnp.einsum('qhd,khd->hqk', queries, keys_block, preferred_element_type=jn...  40.1 us
    all_gather x4, waiting for transfers between devices, gather_in_order(): blocks = lax.all_gather(blocks, axes[k], axis=0, tiled=True)  38.4 us
    all_to_all x1, waiting for transfers between devices, sent_to_all(): lax.all_to_all(jnp.broadcast_to(shard[None], (peers, *shard.shape)), axis...  38.1 us
    all_gather x1, waiting for transfers between devices, gather_axes(): filled = lax.all_gather(filled, axes[number], axis=dim, tiled=True)  23.2 us
    all_to_all x1, starting transfers between devices, summed_on_arrival(): lax.all_to_all(cut_along(shard, dim, peers), axis, 0, 0, tiled=True)  13.6 us
    another operation x32, other arithmetic, weighted_values(): within = lax.cumsum(grouped, axis=3, reverse=True) - grouped  12.2 us
  transfers between devices with their start and end apart: 8, of which 5 were waited for; matrix products, arithmetic and copies ran while one was open for 32% of the time, Pallas kernels for 0%

commit v1 on v0

--- a/solution.py
+++ b/solution.py
@@ -22,7 +22,9 @@
 def gather_in_order(shard, axes, sequence):
     blocks = shard[None]
     for k in sequence:
-        blocks = lax.all_gather(blocks, axes[k], axis=0, tiled=True)
+        blocks = jnp.concatenate(
+            lax.all_to_all(jnp.stack([blocks] * lax.axis_size(axes[k])), axes[k], 0, 0), axis=0
+        )
     carried = [lax.axis_size(axes[k]) for k in reversed(sequence)]
     blocks = blocks.reshape(*carried, *shard.shape)
     turned = sorted(range(len(sequence)), key=lambda place: sequence[len(sequence) - 1 - place])

time: 435 us -> 481 us (1.11)
  blocking collectives: 146 us -> 205 us
  waiting for transfers between devices: 109 us -> 83.4 us
  starting transfers between devices: 19.2 us -> 31 us
    all_to_all x0 -> x9, blocking collectives: none -> 194 us  [gather_in_order(): lax.all_to_all(jnp.stack([blocks] * lax.axis_size(axes[k])), axes[k], 0, 0)]
    all_gather x6 -> x0, blocking collectives: 136 us -> none  [gather_in_order(): blocks = lax.all_gather(blocks, axes[k], axis=0, tiled=True)]
    all_gather x4 -> x0, waiting for transfers between devices: 38.4 us -> none  [gather_in_order(): blocks = lax.all_gather(blocks, axes[k], axis=0, tiled=True)]
    all_to_all x0 -> x1, waiting for transfers between devices: none -> 8.97 us  [gather_in_order(): lax.all_to_all(jnp.stack([blocks] * lax.axis_size(axes[k])), axes[k], 0, 0)]
    all_to_all x1, starting transfers between devices: 5.39 us -> 13.2 us  [sent_to_all(): lax.all_to_all(jnp.broadcast_to(shard[None], (peers, *shard.shape)), axis...]
    transpose x2 -> x0, local copies, waits for them, and re-layouts: 6.51 us -> none  [gather_in_order(): blocks.transpose(*turned, *range(len(sequence), blocks.ndim))]
  transfers between devices with their start and end apart: 8 -> 5, of which waited for: 5 -> 4; matrix products, arithmetic and copies ran while one was open for 32% -> 28% of each run, Pallas kernels for 0% -> 0%
where the time goes in v1:
time: 481 us; the launch traced here: 479 us
  blocking collectives  205 us (43%)
  matrix products  93 us (19%)
  waiting for transfers between devices  83.4 us (17%)
  other arithmetic  33.5 us (7%)
  starting transfers between devices  31 us (6%)
  local copies, waits for them, and re-layouts  18.2 us (4%)
  between operations  13.7 us (3%)
    all_to_all x9, blocking collectives, gather_in_order(): lax.all_to_all(jnp.stack([blocks] * lax.axis_size(axes[k])), axes[k], 0, 0)  194 us
    dot_general x32, matrix products, weighted_values(): jnp.einsum('hqk,khd->qhd', weights, values, preferred_element_type=jnp.fl...  46.6 us
    dot_general x32, matrix products, head_logs(): jnp.einsum('qhd,khd->hqk', queries, keys_block, preferred_element_type=jn...  40.1 us
    all_to_all x1, waiting for transfers between devices, sent_to_all(): lax.all_to_all(jnp.broadcast_to(shard[None], (peers, *shard.shape)), axis...  38.1 us
    all_gather x1, waiting for transfers between devices, gather_axes(): filled = lax.all_gather(filled, axes[number], axis=dim, tiled=True)  26.9 us
    all_to_all x1, starting transfers between devices, summed_on_arrival(): lax.all_to_all(cut_along(shard, dim, peers), axis, 0, 0, tiled=True)  14.1 us
    all_to_all x1, starting transfers between devices, sent_to_all(): lax.all_to_all(jnp.broadcast_to(shard[None], (peers, *shard.shape)), axis...  13.2 us
    another operation x32, other arithmetic, weighted_values(): within = lax.cumsum(grouped, axis=3, reverse=True) - grouped  12.2 us
  transfers between devices with their start and end apart: 5, of which 4 were waited for; matrix products, arithmetic and copies ran while one was open for 28% of the time, Pallas kernels for 0%

profile of v1, /device:TPU:1, one launch (start us, length us, event | category | flops | bytes accessed | tf_op | source)
XLA Modules:
  0.0 479.2 jit_solution(1384306162756783904)
XLA Ops:
  7.3 26.9 %all_to_all.60 = bf16[16,1,128,2]{2,3,1,0:T(2,128)(2,1)S(1)} all-to-all(bf16[16,1,128,2]{2,3,1,0:T(2,128)(2,1)S(1)} %stack.34), channel_id=1, replica_groups=mesh['sp_0'=16,'sp_1'=4,'tp'=8] {'sp_0'}, dimensions={0} | all-to-all | bytes 16384 | tf_op jit(solution)/shard_map/all_to_all | solution.py:26
  34.2 8.3 %all_to_all.61 = bf16[4,16,128,2]{2,1,3,0:T(8,128)(2,1)S(1)} all-to-all(bf16[4,16,128,2]{2,1,3,0:T(8,128)(2,1)S(1)} %stack.35), channel_id=1, replica_groups=mesh['sp_0'=16,'sp_1'=4,'tp'=8] {'sp_1'}, dimensions={0} | all-to-all | bytes 65536 | tf_op jit(solution)/shard_map/all_to_all | solution.py:26
  43.2 15.3 %all_to_all.62 = bf16[16,1,128,64]{2,3,1,0:T(8,128)(2,1)S(1)} all-to-all(bf16[16,1,128,64]{2,3,1,0:T(8,128)(2,1)S(1)} %stack.30), channel_id=1, replica_groups=mesh['sp_0'=16,'sp_1'=4,'tp'=8] {'sp_0'}, dimensions={0} | all-to-all | bytes 524288 | tf_op jit(solution)/shard_map/all_to_all | solution.py:26
  59.3 21.8 %all_to_all.63 = bf16[16,1,128,64]{2,3,1,0:T(8,128)(2,1)S(1)} all-to-all(bf16[16,1,128,64]{2,3,1,0:T(8,128)(2,1)S(1)} %stack.32), channel_id=1, replica_groups=mesh['sp_0'=16,'sp_1'=4,'tp'=8] {'sp_0'}, dimensions={0} | all-to-all | bytes 524288 | tf_op jit(solution)/shard_map/all_to_all | solution.py:26
  81.4 12.9 %all_to_all.64 = bf16[4,16,128,64]{2,3,1,0:T(8,128)(2,1)} all-to-all(bf16[4,16,128,64]{2,3,1,0:T(8,128)(2,1)S(1)} %stack.31), channel_id=1, replica_groups=mesh['sp_0'=16,'sp_1'=4,'tp'=8] {'sp_1'}, dimensions={0} | all-to-all | bytes 2097152 | tf_op jit(solution)/shard_map/all_to_all | solution.py:26
  94.5 12.9 %all_to_all.65 = bf16[4,16,128,64]{2,3,1,0:T(8,128)(2,1)} all-to-all(bf16[4,16,128,64]{2,3,1,0:T(8,128)(2,1)S(1)} %stack.33), channel_id=1, replica_groups=mesh['sp_0'=16,'sp_1'=4,'tp'=8] {'sp_1'}, dimensions={0} | all-to-all | bytes 2097152 | tf_op jit(solution)/shard_map/all_to_all | solution.py:26
  107.5 39.2 %all_to_all.66 = bf16[16,1,128,128]{3,2,1,0:T(8,128)(2,1)S(1)} all-to-all(bf16[16,1,128,128]{3,2,1,0:T(8,128)(2,1)S(1)} %stack.36), channel_id=1, replica_groups=mesh['sp_0'=16,'sp_1'=4,'tp'=8] {'sp_0'}, dimensions={0} | all-to-all | bytes 1048576 | tf_op jit(solution)/shard_map/all_to_all | solution.py:26
  146.8 33.9 %all_to_all.67 = bf16[16,1,128,128]{3,2,1,0:T(8,128)(2,1)S(1)} all-to-all(bf16[16,1,128,128]{3,2,1,0:T(8,128)(2,1)S(1)} %stack.38), channel_id=1, replica_groups=mesh['sp_0'=16,'sp_1'=4,'tp'=8] {'sp_0'}, dimensions={0} | all-to-all | bytes 1048576 | tf_op jit(solution)/shard_map/all_to_all | solution.py:26
  181.2 23.0 %all_to_all.68 = bf16[4,16,128,128]{3,2,1,0:T(8,128)(2,1)} all-to-all(bf16[4,16,128,128]{3,2,1,0:T(8,128)(2,1)S(1)} %stack.37), channel_id=1, replica_groups=mesh['sp_0'=16,'sp_1'=4,'tp'=8] {'sp_1'}, dimensions={0} | all-to-all | bytes 4194304 | tf_op jit(solution)/shard_map/all_to_all | solution.py:26
  206.2 3.7 all-to-all-start.9
  210.8 2.8 copy.37
  213.6 2.7 copy.38
  216.4 3.2 copy.33
  219.6 9.0 %all-to-all-done.9 = bf16[4,16,128,128]{3,2,1,0:T(8,128)(2,1)S(1)} async-done(((bf16[4,16,128,128]{3,2,1,0:T(8,128)(2,1)}), bf16[4,16,128,128]{3,2,1,0:T(8,128)(2,1)S(1)}, u32[]{:S(2)}, u32[]{:S(2)}) %all-to-all-start.9) | async-done | bytes 2097184 | tf_op jit(solution)/shard_map/all_to_all | solution.py:26
  230.0 116.7 %while.20 = (s32[]{:T(128)}, f32[128,1,64]{0,2,1:T(8,128)S(1)}, f32[128,1,128]{0,2,1:T(8,128)S(1)}, f32[1,128]{1,0:T(1,128)S(1)}, f32[1,128]{1,0:T(1,128)S(1)}, ...) while((s32[]{:T(128)}, f32[128,1,64]{0,2,1:T(8,128)S(1)}, ...), condition=%wide.region_9.10_spmd.clone, body=%wide.region_0.9_spmd.clone.sunk | while | flops 57983880 | bytes 5200671 | solution.py:190
  347.4 2.5 broadcast_in_dim.49
  349.9 13.2 %all-to-all-start.10 = ((bf16[8,128,2048]{2,1,0:T(8,128)(2,1)}), bf16[8,128,2048]{2,1,0:T(8,128)(2,1)}, u32[]{:S(2)}, u32[]{:S(2)}) async-start(bf16[8,128,2048]{2,1,0:T(8,128)(2,1)} %broadcast_in_dim.49), calls=%async_computation.10 | async-start | bytes 8388608 | tf_op jit(solution)/shard_map/all_to_all | solution.py:40
  363.1 10.7 %all_gather.10 = bf16[384,128]{0,1:T(8,128)(2,1)} all-gather(bf16[384,32]{0,1:T(8,128)(2,1)S(1)} %copy-done.8), channel_id=1, replica_groups=mesh['sp_0'=16,'sp_1'=4,'tp'=8] {'sp_1'}, dimensions={1}, use_global_device_ids=true | all-gather | bytes 122880 | tf_op jit(solution)/shard_map/all_gather | solution.py:59
  373.8 38.1 %all-to-all-done.10 = bf16[8,128,2048]{2,1,0:T(8,128)(2,1)} async-done(((bf16[8,128,2048]{2,1,0:T(8,128)(2,1)}), bf16[8,128,2048]{2,1,0:T(8,128)(2,1)}, u32[]{:S(2)}, u32[]{:S(2)}) %all-to-all-start.10) | async-done | bytes 4194336 | tf_op jit(solution)/shard_map/all_to_all | solution.py:40
  411.9 3.0 convert_reduce_fusion
  417.6 26.9 %all-gather.5.cloned.1.call-done = bf16[384,2048]{0,1:T(8,128)(2,1)} async-done(((bf16[384,128]{0,1:T(8,128)(2,1)}), bf16[384,2048]{0,1:T(8,128)(2,1)}) %all-gather.5.cloned.1.call-update) | async-done | bytes 1572880 | tf_op jit(solution)/shard_map/all_gather | solution.py:59
  444.5 3.7 convolution_convert_fusion
  448.2 14.1 %all-to-all-start.11 = ((bf16[8,16,2048]{2,1,0:T(8,128)(2,1)}), bf16[8,16,2048]{2,1,0:T(8,128)(2,1)S(1)}, u32[]{:S(2)}, u32[]{:S(2)}) async-start(bf16[8,16,2048]{2,1,0:T(8,128)(2,1)} %bitcast.18), calls=%async_computation.11 | async-start | bytes 1048576 | tf_op jit(solution)/shard_map/all_to_all | solution.py:71
  462.2 9.3 %all-to-all-done.11 = bf16[8,16,2048]{2,1,0:T(8,128)(2,1)S(1)} async-done(((bf16[8,16,2048]{2,1,0:T(8,128)(2,1)}), bf16[8,16,2048]{2,1,0:T(8,128)(2,1)S(1)}, u32[]{:S(2)}, u32[]{:S(2)}) %all-to-all-start.11) | async-done | bytes 524320 | tf_op jit(solution)/shard_map/all_to_all | solution.py:71
  (311 shorter events, 126.8 us)
Async XLA Ops:
  6.5 340.5 %copy-start = (bf16[128,2048]{1,0:T(8,128)(2,1)S(1)}, bf16[128,2048]{1,0:T(8,128)(2,1)}, u32[]{:S(2)}) copy-start(bf16[128,2048]{1,0:T(8,128)(2,1)} %param.25) | copy-start | bytes 1572868
  94.3 13.1 %copy-start.4 = (bf16[128,128]{1,0:T(8,128)(2,1)S(1)}, bf16[128,128]{1,0:T(8,128)(2,1)}, u32[]{:S(2)}) copy-start(bf16[128,128]{1,0:T(8,128)(2,1)} %param.22) | copy-start | bytes 98308
  94.5 52.2 %copy-start.5 = (bf16[128,128]{1,0:T(8,128)(2,1)S(1)}, bf16[128,128]{1,0:T(8,128)(2,1)}, u32[]{:S(2)}) copy-start(bf16[128,128]{1,0:T(8,128)(2,1)} %param.20) | copy-start | bytes 98308
  206.2 3.8 copy-start.6
  206.2 3.8 copy-start.7
  206.2 22.3 %all-to-all-start.9 = ((bf16[4,16,128,128]{3,2,1,0:T(8,128)(2,1)}), bf16[4,16,128,128]{3,2,1,0:T(8,128)(2,1)S(1)}, u32[]{:S(2)}, u32[]{:S(2)}) async-start(bf16[4,16,128,128]{3,2,1,0:T(8,128)(2,1)} %stack.39), calls=%async_computation.9 | async-start | bytes 4194304 | tf_op jit(solution)/shard_map/all_to_all | solution.py:26
  209.9 205.3 %all-gather.3.cloned.1.call-start = ((), (), s32[]{:S(2)}) async-start(), calls=%async_computation.12 | async-start | bytes 3194880 | tf_op jit(solution)/shard_map/all_gather | solution.py:52
  219.5 10.5 %copy-start.2 = (bf16[128,64]{0,1:T(8,128)(2,1)S(1)}, bf16[128,64]{0,1:T(8,128)(2,1)}, u32[]{:S(2)}) copy-start(bf16[128,64]{0,1:T(8,128)(2,1)} %param.17) | copy-start | bytes 49156
  219.6 10.5 %copy-start.9 = (bf16[128,128]{1,0:T(8,128)(2,1)S(1)}, bf16[128,128]{1,0:T(8,128)(2,1)}, u32[]{:S(2)}) copy-start(bf16[128,128]{1,0:T(8,128)(2,1)} %param.18) | copy-start | bytes 98308
  230.0 116.7 %copy-start.3 = (bf16[64,2048]{1,0:T(8,128)(2,1)S(1)}, bf16[64,2048]{1,0:T(8,128)(2,1)}, u32[]{:S(2)}) copy-start(bf16[64,2048]{1,0:T(8,128)(2,1)} %param.24) | copy-start | bytes 786436
  349.9 13.2 %copy-start.8 = (bf16[384,32]{0,1:T(8,128)(2,1)S(1)}, bf16[384,32]{0,1:T(8,128)(2,1)}, u32[]{:S(2)}) copy-start(bf16[384,32]{0,1:T(8,128)(2,1)} %param.29) | copy-start | bytes 73732
  349.9 62.0 %all-to-all-start.10 = ((bf16[8,128,2048]{2,1,0:T(8,128)(2,1)}), bf16[8,128,2048]{2,1,0:T(8,128)(2,1)}, u32[]{:S(2)}, u32[]{:S(2)}) async-start(bf16[8,128,2048]{2,1,0:T(8,128)(2,1)} %broadcast_in_dim.49), calls=%async_computation.10 | async-start | bytes 8388608 | tf_op jit(solution)/shard_map/all_to_all | solution.py:40
  363.1 81.4 %all-gather.5.cloned.1.call-start = ((), (), s32[]{:S(2)}) async-start(), calls=%async_computation.13 | async-start | bytes 1671168 | tf_op jit(solution)/shard_map/all_gather | solution.py:59
  373.8 41.1 %copy-start.1 = (bf16[128,2048]{1,0:T(8,128)(2,1)S(1)}, bf16[128,2048]{1,0:T(8,128)(2,1)}, u32[]{:S(2)}) copy-start(bf16[128,2048]{1,0:T(8,128)(2,1)} %param.16) | copy-start | bytes 1572868
  415.0 0.7 copy-start.10
  448.2 23.4 %all-to-all-start.11 = ((bf16[8,16,2048]{2,1,0:T(8,128)(2,1)}), bf16[8,16,2048]{2,1,0:T(8,128)(2,1)S(1)}, u32[]{:S(2)}, u32[]{:S(2)}) async-start(bf16[8,16,2048]{2,1,0:T(8,128)(2,1)} %bitcast.18), calls=%async_computation.11 | async-start | bytes 1048576 | tf_op jit(solution)/shard_map/all_to_all | solution.py:71
Sparse Core Ops, SparseCore 0:
  213.7 143.9 all-gather.2
  373.9 70.4 all-gather.4
